TPU v7x, 32 devices: a whole 2x2x4 slice. The times are simulated.
32 devices in a mesh: ep: 32 (over z, y, x, core).
Axes of the slice: x: 2, y: 2, z: 4, core: 2. Of those that a mesh axis runs over, the one named last changes fastest.
Arguments:
- tokens: bfloat16 [2048, 2048], P('ep'), may hold values from -6 to 6
- conv_state: bfloat16 [2048, 3, 1024], P('ep'), may hold values from -6 to 6
- recur_state: float32 [2048, 1024], P('ep'), may hold values from -6 to 6
- w_branch: bfloat16 [2048, 1024], replicated, may hold values from -0.125 to 0.125
- w_gate: bfloat16 [2048, 1024], replicated, may hold values from -0.125 to 0.125
- conv_taps: float32 [4, 1024], replicated, may hold values from -3 to 3
- rate_blocks: bfloat16 [16, 64, 64], replicated, may hold values from -0.75 to 0.75
- input_blocks: bfloat16 [16, 64, 64], replicated, may hold values from -0.75 to 0.75
- decay_param: float32 [1024], replicated, may hold values from 1.5 to 6.5
- w_mix: bfloat16 [1024, 2048], replicated, may hold values from -0.1875 to 0.1875
- gain_pre: float32 [2048], replicated, may hold values from 0.1 to 1.9
- gain_post: float32 [2048], replicated, may hold values from 0.1 to 1.9
- gain_ffn: float32 [2048], replicated, may hold values from 0.1 to 1.9
- gain_out: float32 [2048], replicated, may hold values from 0.1 to 1.9
- routes: int32 [2048, 2], P('ep'), may hold values from 0 to 31, all different within a row; in each aligned block of 64 rows (0 to 63, 64 to 127, ...) at most 12 rows name the same one
- affinity: float32 [2048, 2], P('ep'), may hold values from 0.05 to 1
- w_expert_gate: bfloat16 [32, 2048, 512], P('ep'), may hold values from -0.125 to 0.125
- w_expert_up: bfloat16 [32, 2048, 512], P('ep'), may hold values from -0.125 to 0.125
- w_expert_down: bfloat16 [32, 512, 2048], P('ep'), may hold values from -0.25 to 0.25
Outputs:
- layer_out: bfloat16 [2048, 2048], P('ep')
- conv_next: bfloat16 [2048, 3, 1024], P('ep')
- state_next: float32 [2048, 1024], P('ep')
Inputs may be any that keep to these rules, and one draw needn't show every extreme that they name: `routes`: each row names 2 different experts. Among the 64 rows of one device no expert is named more than 12 times, and in every draw some device names some expert exactly 12 times.
All inputs are finite; a program needn't handle non-finite values.
Results may differ from a plain program's by a relative error of at most 0.014.
Values may be sent and summed in bfloat16 or wider, within the bound.
A program may use at most 128 MiB of HBM per device.

v0:
```python
import jax
import jax.numpy as jnp
from jax import lax
from jax.sharding import PartitionSpec as P

epsilon = 1e-06
gate_scale = 8.0


def norm_rows(values, gain_vec):
    floats = values.astype(jnp.float32)
    inv_scale = lax.rsqrt(jnp.mean(floats * floats, axis=-1, keepdims=True) + epsilon)
    return floats * inv_scale * gain_vec


def recurrence(
    tokens,
    conv_state,
    recur_state,
    w_branch,
    w_gate,
    conv_taps,
    rate_blocks,
    input_blocks,
    decay_param,
    w_mix,
    gain_pre,
    gain_post,
):
    normed = norm_rows(tokens, gain_pre).astype(jnp.bfloat16)
    branch = jnp.dot(normed, w_branch, preferred_element_type=jnp.float32).astype(jnp.bfloat16)
    gate_act = jnp.dot(normed, w_gate, preferred_element_type=jnp.float32).astype(jnp.bfloat16)
    window = jnp.concatenate([conv_state, branch[:, None, :]], axis=1)
    convolved = jnp.sum(window.astype(jnp.float32) * conv_taps[None], axis=1)
    row_count, branch_width = convolved.shape
    blocks = rate_blocks.shape[0]
    pieces = convolved.reshape(row_count, blocks, branch_width // blocks)
    rate_gate = jax.nn.sigmoid(
        jnp.einsum("snc,ncd->snd", pieces, rate_blocks.astype(jnp.float32)).reshape(
            row_count, branch_width
        )
    )
    inflow = jax.nn.sigmoid(
        jnp.einsum("snc,ncd->snd", pieces, input_blocks.astype(jnp.float32)).reshape(
            row_count, branch_width
        )
    )
    log_decay = -gate_scale * rate_gate * jax.nn.softplus(-decay_param)
    state_next = jnp.exp(log_decay) * recur_state + jnp.sqrt(-jnp.expm1(2.0 * log_decay)) * (
        inflow * convolved
    )
    merged = (state_next * jax.nn.gelu(gate_act.astype(jnp.float32))).astype(jnp.bfloat16)
    mix_out = jnp.dot(merged, w_mix, preferred_element_type=jnp.float32).astype(jnp.bfloat16)
    residual = tokens.astype(jnp.float32) + norm_rows(mix_out, gain_post)
    return (residual, window[:, 1:, :], state_next)


def expert_block(got_rows, got_info, cap_total, w_expert_gate, w_expert_up, w_expert_down):
    slot_count, sources, model_width = got_rows.shape
    counts = got_info[0]
    before = jnp.cumsum(counts) - counts
    allowed = jnp.clip(cap_total - before, 0, counts)
    positions = jnp.arange(slot_count, dtype=jnp.int32)
    keep_mask = positions[:, None] < allowed[None, :]
    row_block = got_rows.reshape(slot_count * sources, model_width)
    gate_part = jnp.dot(row_block, w_expert_gate[0], preferred_element_type=jnp.float32)
    up_part = jnp.dot(row_block, w_expert_up[0], preferred_element_type=jnp.float32)
    hidden = (jax.nn.silu(gate_part) * up_part).astype(jnp.bfloat16)
    outputs = jnp.dot(hidden, w_expert_down[0], preferred_element_type=jnp.float32).astype(
        jnp.bfloat16
    )
    outputs = outputs.reshape(slot_count, sources, model_width)
    return jnp.where(keep_mask[:, :, None], outputs, jnp.zeros_like(outputs))


def shards(
    tokens,
    conv_state,
    recur_state,
    w_branch,
    w_gate,
    conv_taps,
    rate_blocks,
    input_blocks,
    decay_param,
    w_mix,
    gain_pre,
    gain_post,
    gain_ffn,
    gain_out,
    routes,
    affinity,
    w_expert_gate,
    w_expert_up,
    w_expert_down,
):
    residual, conv_next, state_next = recurrence(
        tokens,
        conv_state,
        recur_state,
        w_branch,
        w_gate,
        conv_taps,
        rate_blocks,
        input_blocks,
        decay_param,
        w_mix,
        gain_pre,
        gain_post,
    )
    ffn_in = norm_rows(residual, gain_ffn).astype(jnp.bfloat16)
    seq_count, top_count = routes.shape
    model_width = ffn_in.shape[1]
    experts = lax.axis_size("ep") * w_expert_gate.shape[0]
    capacity = max(2, 3 * seq_count * top_count // lax.axis_size("ep"))
    cap_total = seq_count * top_count // 2
    flat_routes = routes.reshape(-1)
    onehot = (flat_routes[:, None] == jnp.arange(experts, dtype=jnp.int32)[None, :]).astype(
        jnp.int32
    )
    slot_index = jnp.sum(jnp.cumsum(onehot, axis=0) * onehot, axis=1) - 1
    load_counts = jnp.sum(onehot, axis=0)
    slot_target = slot_index * experts + flat_routes
    outgoing = (
        jnp.zeros((capacity * experts, model_width), jnp.bfloat16)
        .at[slot_target]
        .set(jnp.repeat(ffn_in, top_count, axis=0))
    )
    outgoing = outgoing.reshape(capacity, experts, model_width)
    send_info = load_counts[None, :]
    got_rows, got_info = (
        lax.all_to_all(outgoing, "ep", split_axis=1, concat_axis=1, tiled=True),
        lax.all_to_all(send_info, "ep", split_axis=1, concat_axis=1, tiled=True),
    )
    finished = expert_block(
        got_rows, got_info, cap_total, w_expert_gate, w_expert_up, w_expert_down
    )
    gathered = lax.all_to_all(finished, "ep", split_axis=1, concat_axis=1, tiled=True)
    picked = jnp.take(gathered.reshape(capacity * experts, model_width), slot_target, axis=0)
    picked = picked.astype(jnp.float32).reshape(seq_count, top_count, model_width)
    weights = affinity / jnp.sum(affinity, axis=1, keepdims=True)
    combined = jnp.sum(weights[:, :, None] * picked, axis=1)
    layer_out = (residual + norm_rows(combined, gain_out)).astype(jnp.bfloat16)
    return (layer_out, conv_next, state_next)


def solution(mesh):
    return jax.shard_map(
        shards,
        mesh=mesh,
        in_specs=(
            P("ep", None),
            P("ep", None, None),
            P("ep", None),
            P(),
            P(),
            P(),
            P(),
            P(),
            P(),
            P(),
            P(),
            P(),
            P(),
            P(),
            P("ep", None),
            P("ep", None),
            P("ep", None, None),
            P("ep", None, None),
            P("ep", None, None),
        ),
        out_specs=(P("ep", None), P("ep", None, None), P("ep", None)),
        check_vma=False,
    )
```

profile of v0, /device:TPU:0, one launch (start us, length us, event | category | flops | bytes accessed | tf_op | source)
XLA Modules:
  0.0 170.9 jit_solution(7606808229073026035)
XLA Ops:
  0.6 0.0 copy-start
  0.6 0.9 copy.69
  1.6 0.1 eq.15
  1.7 0.1 fusion.54
  1.8 0.2 reduce_window_sum.18
  2.0 0.7 fusion.55
  2.7 0.7 copy.72
  3.4 7.3 %all-to-all-start = ((s32[1,32,1]{2,0,1:T(1,128)}), s32[1,32,1]{2,0,1:T(1,128)S(1)}, u32[]{:S(2)}, u32[]{:S(2)}) async-start(s32[1,32,1]{2,0,1:T(1,128)} %copy.72), calls=%async_computation | async-start | bytes 32768 | tf_op jit(solution)/shard_map/all_to_all | solution.py:133
  10.7 0.7 reshape.196
  11.4 1.1 fusion.31
  12.5 0.0 copy-start.3
  12.5 0.0 copy-start.9
  12.5 0.0 copy-start.22
  12.5 3.2 %fusion.21 = bf16[64,1,1024]{2,0,1:T(8,128)(2,1)S(1)} fusion(bf16[2048,1024]{1,0:T(8,128)(2,1)} %param.22, bf16[64,2048]{1,0:T(8,128)(2,1)} %param.19, f32[2048]{0:T(1024)} %param.29, f32[64]{0:T(128)S(1)} %add_rsqrt_fusion.3), kind=kOutput, calls=%fused_computation.26 | convolution fusion | flops 269025280 | bytes 4595968 | tf_op jit(solution)/shard_map/dot_general | solution.py:31
  15.8 0.1 multiply_reduce_fusion.1
  15.9 0.2 reshape.193
  16.1 0.3 fusion.16
  16.4 0.3 copy.65
  16.7 0.2 div.38
  16.9 1.2 fusion.19
  18.2 0.0 copy-start.1
  18.2 0.3 copy.67
  18.5 0.9 div.40
  19.4 0.7 fusion.56
  20.1 1.3 multiply_add_fusion
  21.3 0.0 copy-start.5
  21.4 0.0 copy-start.7
  21.4 0.0 copy-start.10
  21.4 0.0 copy-start.19
  21.4 5.3 %multiply_reduce_fusion.4 = (f32[64]{0:T(128)S(1)}, f32[64,2048]{1,0:T(8,128)S(1)}) fusion(bf16[1024,2048]{1,0:T(8,128)(2,1)} %param.28, f32[64,1024]{1,0:T(8,128)S(1)} %multiply_add_fusion, bf16[2048,1024]{1,0:T(8,128)(2,1)} %param.23, bf16[64,2048]{1,0:T(8,128)(2,1)S(1)} %copy-done.1, f32[2048]{0:T(1024)} %param.29, f32[64]{0:T(128)} %copy-done.16), kind=kOutput, calls=%fused_computation.50 | convolution fusion | flops 538705856 | bytes 9445888 | tf_op jit(solution)/shard_map/dot_general | solution.py:53
  26.8 0.3 multiply_reduce_fusion.3
  27.1 0.2 multiply_convert_fusion
  27.3 0.0 copy-done.12
  27.3 0.5 fusion.57
  27.8 0.3 broadcast_in_dim.30
  28.1 1.0 reshape.214
  29.1 3.2 %scatter_custom_fusion = bf16[384,2048]{1,0:T(8,128)(2,1)} fusion(s32[128]{0:T(128)} %fusion.57, bf16[128,2048]{1,0:T(8,128)(2,1)} %reshape.214, bf16[]{:T(256)} %constant.60.clone.1), kind=kCustom, calls=%fused_computation.35 | custom fusion | bytes 1573376 | tf_op jit(solution)/shard_map/scatter | solution.py:127
  32.4 3.7 %copy.75 = bf16[12,32,2048]{2,0,1:T(8,128)(2,1)} copy(bf16[12,32,2048]{2,1,0:T(8,128)(2,1)} %bitcast.41) | data formatting | bytes 3145728 | tf_op jit(solution)/shard_map/reshape | solution.py:129
  36.0 6.1 %all-to-all-start.1 = ((bf16[12,32,2048]{2,0,1:T(8,128)(2,1)}), bf16[12,32,2048]{2,0,1:T(8,128)(2,1)}, u32[]{:S(2)}, u32[]{:S(2)}) async-start(bf16[12,32,2048]{2,0,1:T(8,128)(2,1)} %copy.75), calls=%async_computation.1 | async-start | bytes 4194304 | tf_op jit(solution)/shard_map/all_to_all | solution.py:132
  42.2 0.1 reduce-window.8
  42.2 0.1 reduce.1
  42.4 0.7 reduce
  43.0 0.1 iota_compare_fusion.1
  43.1 47.7 %all-to-all-done.1 = bf16[12,32,2048]{2,0,1:T(8,128)(2,1)} async-done(((bf16[12,32,2048]{2,0,1:T(8,128)(2,1)}), bf16[12,32,2048]{2,0,1:T(8,128)(2,1)}, u32[]{:S(2)}, u32[]{:S(2)}) %all-to-all-start.1) | async-done | bytes 1572896 | tf_op jit(solution)/shard_map/all_to_all | solution.py:132
  90.8 2.6 %copy.76 = bf16[12,32,2048]{2,1,0:T(8,128)(2,1)S(1)} copy(bf16[12,32,2048]{2,0,1:T(8,128)(2,1)} %all-to-all-done.1) | data formatting | bytes 3145728 | tf_op jit(solution)/shard_map/all_to_all | solution.py:132
  93.5 1.1 copy-done.2
  94.6 1.9 %fusion.4 = f32[384,512]{1,0:T(8,128)} fusion(bf16[384,2048]{1,0:T(8,128)(2,1)S(1)} %bitcast.42, bf16[1,2048,512]{2,1,0:T(8,128)(2,1)S(1)} %copy-done.21), kind=kOutput, calls=%fused_computation.8 | convolution fusion | flops 805306368 | bytes 4456448 | tf_op jit(solution)/shard_map/dot_general | solution.py:66
  96.5 5.3 %convolution_convert_fusion = bf16[384,2048]{1,0:T(8,128)(2,1)} fusion(bf16[1,512,2048]{2,1,0:T(8,128)(2,1)S(1)} %copy-done, bf16[384,2048]{1,0:T(8,128)(2,1)} %bitcast.43, bf16[1,2048,512]{2,1,0:T(8,128)(2,1)} %param.36, f32[384,512]{1,0:T(8,128)} %fusion.4), kind=kOutput, calls=%fused_computation.2 | convolution fusion | flops 1612578816 | bytes 8126464 | tf_op jit(solution)/shard_map/dot_general | solution.py:69
  101.8 3.7 %copy_select_fusion = bf16[12,32,2048]{2,0,1:T(8,128)(2,1)} fusion(bf16[12,32,2048]{2,1,0:T(8,128)(2,1)} %bitcast.44, pred[12,32]{0,1:T(8,128)(4,1)S(1)} %iota_compare_fusion.1), kind=kLoop, calls=%fused_computation.10 | loop fusion | flops 786432 | bytes 3146112 | tf_op jit(solution)/shard_map/jit(_where)/select_n | solution.py:73
  105.4 0.0 copy-start.4
  105.5 4.1 %all-to-all-start.2 = ((bf16[12,32,2048]{2,0,1:T(8,128)(2,1)}), bf16[12,32,2048]{2,0,1:T(8,128)(2,1)}, u32[]{:S(2)}, u32[]{:S(2)}) async-start(bf16[12,32,2048]{2,0,1:T(8,128)(2,1)} %copy_select_fusion), calls=%async_computation.2 | async-start | bytes 4194304 | tf_op jit(solution)/shard_map/all_to_all | solution.py:138
  109.6 0.1 mul.210
  109.7 0.1 copy.70
  109.8 0.1 copy.71
  110.0 0.7 copy.68
  110.7 0.8 fusion.36
  111.5 46.8 %all-to-all-done.2 = bf16[12,32,2048]{2,0,1:T(8,128)(2,1)} async-done(((bf16[12,32,2048]{2,0,1:T(8,128)(2,1)}), bf16[12,32,2048]{2,0,1:T(8,128)(2,1)}, u32[]{:S(2)}, u32[]{:S(2)}) %all-to-all-start.2) | async-done | bytes 1572896 | tf_op jit(solution)/shard_map/all_to_all | solution.py:138
  158.3 3.6 %copy.78 = bf16[12,32,2048]{2,1,0:T(8,128)(2,1)} copy(bf16[12,32,2048]{2,0,1:T(8,128)(2,1)} %all-to-all-done.2) | data formatting | bytes 3145728 | tf_op jit(solution)/shard_map/all_to_all | solution.py:138
  161.9 3.1 %gather_fusion = bf16[128,2048]{1,0:T(8,128)(2,1)S(1)} fusion(bf16[384,2048]{1,0:T(8,128)(2,1)} %bitcast.40, s32[1024]{0:T(1024)S(1)} %pad_clamp_fusion), kind=kCustom, calls=%fused_computation | custom fusion | bytes 1049088 | tf_op jit(solution)/shard_map/jit(_take)/gather | solution.py:139
  165.0 0.0 copy-start.11
  165.0 1.1 gather.7
  166.1 3.7 %multiply_reduce_fusion = f32[64,2048]{1,0:T(8,128)S(1)} fusion(bf16[64,2,2048]{2,1,0:T(2,128)(2,1)} %gather.7, pred[64,2]{1,0:T(8,128)(4,1)S(1)} %copy.71, f32[64,2]{1,0:T(8,128)S(1)} %copy-done.6), kind=kLoop, calls=%fused_computation.27 | loop fusion | flops 917504 | bytes 1049216 | tf_op jit(solution)/shard_map/reduce_sum | solution.py:142
  169.8 0.1 multiply_reduce_fusion.2
  170.0 0.9 add_convert_fusion
  (44 shorter events, 0.2 us)
Async XLA Ops:
  0.6 95.8 %copy-start = (bf16[1,512,2048]{2,1,0:T(8,128)(2,1)S(1)}, bf16[1,512,2048]{2,1,0:T(8,128)(2,1)}, u32[]{:S(2)}) copy-start(bf16[1,512,2048]{2,1,0:T(8,128)(2,1)} %param.37) | copy-start | bytes 6291460
  3.4 32.6 %all-to-all-start = ((s32[1,32,1]{2,0,1:T(1,128)}), s32[1,32,1]{2,0,1:T(1,128)S(1)}, u32[]{:S(2)}, u32[]{:S(2)}) async-start(s32[1,32,1]{2,0,1:T(1,128)} %copy.72), calls=%async_computation | async-start | bytes 32768 | tf_op jit(solution)/shard_map/all_to_all | solution.py:133
  12.5 3.3 %copy-start.16 = (f32[64]{0:T(128)}, f32[64]{0:T(128)S(1)}, u32[]{:S(2)}) copy-start(f32[64]{0:T(128)S(1)} %add_rsqrt_fusion.3) | copy-start | bytes 772
  12.5 3.3 %copy-start.3 = (bf16[64,3,1024]{2,0,1:T(8,128)(2,1)S(1)}, bf16[64,3,1024]{2,0,1:T(8,128)(2,1)}, u32[]{:S(2)}) copy-start(bf16[64,3,1024]{2,0,1:T(8,128)(2,1)} %param.20) | copy-start | bytes 1179652
  12.5 3.3 %copy-start.9 = (f32[4,1024]{1,0:T(4,128)S(1)}, f32[4,1024]{1,0:T(4,128)}, u32[]{:S(2)}) copy-start(f32[4,1024]{1,0:T(4,128)} %param.24) | copy-start | bytes 49156
  12.5 3.6 %copy-start.22 = (bf16[16,64,64]{2,1,0:T(8,128)(2,1)S(1)}, bf16[16,64,64]{2,1,0:T(8,128)(2,1)}, u32[]{:S(2)}) copy-start(bf16[16,64,64]{2,1,0:T(8,128)(2,1)} %param.25) | copy-start | bytes 393220
  18.2 3.2 %copy-start.1 = (bf16[64,2048]{1,0:T(8,128)(2,1)S(1)}, bf16[64,2048]{1,0:T(8,128)(2,1)}, u32[]{:S(2)}) copy-start(bf16[64,2048]{1,0:T(8,128)(2,1)} %param.19) | copy-start | bytes 786436
  21.3 5.4 %copy-start.5 = (f32[64,1024]{1,0:T(8,128)}, f32[64,1024]{1,0:T(8,128)S(1)}, u32[]{:S(2)}) copy-start(f32[64,1024]{1,0:T(8,128)S(1)} %multiply_add_fusion) | copy-start | bytes 786436
  21.4 5.4 %copy-start.7 = (f32[2048]{0:T(1024)S(1)}, f32[2048]{0:T(1024)}, u32[]{:S(2)}) copy-start(f32[2048]{0:T(1024)} %param.30) | copy-start | bytes 24580
  21.4 5.7 %copy-start.10 = (f32[2048]{0:T(1024)S(1)}, f32[2048]{0:T(1024)}, u32[]{:S(2)}) copy-start(f32[2048]{0:T(1024)} %param.31) | copy-start | bytes 24580
  21.4 5.9 %copy-start.17 = (s32[128]{0:T(128)S(1)}, s32[128]{0:T(128)}, u32[]{:S(2)}) copy-start(s32[128]{0:T(128)} %get-tuple-element.4) | copy-start | bytes 1540
  21.4 5.9 %copy-start.19 = (s32[128,1]{0,1:T(1,128)S(1)}, s32[128,1]{0,1:T(1,128)}, u32[]{:S(2)}) copy-start(s32[128,1]{0,1:T(1,128)} %reshape.196) | copy-start | bytes 1540
  26.8 0.5 copy-start.12
  36.0 54.8 %all-to-all-start.1 = ((bf16[12,32,2048]{2,0,1:T(8,128)(2,1)}), bf16[12,32,2048]{2,0,1:T(8,128)(2,1)}, u32[]{:S(2)}, u32[]{:S(2)}) async-start(bf16[12,32,2048]{2,0,1:T(8,128)(2,1)} %copy.75), calls=%async_computation.1 | async-start | bytes 4194304 | tf_op jit(solution)/shard_map/all_to_all | solution.py:132
  90.8 3.8 %copy-start.21 = (bf16[1,2048,512]{2,1,0:T(8,128)(2,1)S(1)}, bf16[1,2048,512]{2,1,0:T(8,128)(2,1)}, u32[]{:S(2)}) copy-start(bf16[1,2048,512]{2,1,0:T(8,128)(2,1)} %param.35) | copy-start | bytes 6291460
  93.5 1.1 copy-start.2
  105.4 4.1 %copy-start.18 = (s32[128]{0:T(128)S(1)}, s32[128]{0:T(128)}, u32[]{:S(2)}) copy-start(s32[128]{0:T(128)} %get-tuple-element.4) | copy-start | bytes 1540
  105.4 4.4 %copy-start.14 = (s32[64,2]{0,1:T(2,128)S(1)}, s32[64,2]{0,1:T(2,128)}, u32[]{:S(2)}) copy-start(s32[64,2]{0,1:T(2,128)} %param.33) | copy-start | bytes 1540
  105.4 4.5 %copy-start.15 = (f32[64,2]{0,1:T(2,128)S(1)}, f32[64,2]{0,1:T(2,128)}, u32[]{:S(2)}) copy-start(f32[64,2]{0,1:T(2,128)} %param.34) | copy-start | bytes 1540
  105.4 5.3 %copy-start.20 = (s32[128]{0:T(128)S(1)}, s32[128]{0:T(128)}, u32[]{:S(2)}) copy-start(s32[128]{0:T(128)} %fusion.57) | copy-start | bytes 1540
  105.4 5.3 %copy-start.4 = (bf16[64,3,1024]{2,0,1:T(8,128)(2,1)S(1)}, bf16[64,3,1024]{2,0,1:T(8,128)(2,1)}, u32[]{:S(2)}) copy-start(bf16[64,3,1024]{2,0,1:T(8,128)(2,1)} %param.20) | copy-start | bytes 1179652
  105.5 52.8 %all-to-all-start.2 = ((bf16[12,32,2048]{2,0,1:T(8,128)(2,1)}), bf16[12,32,2048]{2,0,1:T(8,128)(2,1)}, u32[]{:S(2)}, u32[]{:S(2)}) async-start(bf16[12,32,2048]{2,0,1:T(8,128)(2,1)} %copy_select_fusion), calls=%async_computation.2 | async-start | bytes 4194304 | tf_op jit(solution)/shard_map/all_to_all | solution.py:138
  161.9 4.2 %copy-start.6 = (f32[64,2]{1,0:T(8,128)S(1)}, f32[64,2]{1,0:T(8,128)}, u32[]{:S(2)}) copy-start(f32[64,2]{1,0:T(8,128)} %copy.68) | copy-start | bytes 1540
  165.0 5.0 %copy-start.8 = (f32[2048]{0:T(1024)S(1)}, f32[2048]{0:T(1024)}, u32[]{:S(2)}) copy-start(f32[2048]{0:T(1024)} %param.30) | copy-start | bytes 24580
  165.0 5.0 %copy-start.11 = (f32[2048]{0:T(1024)S(1)}, f32[2048]{0:T(1024)}, u32[]{:S(2)}) copy-start(f32[2048]{0:T(1024)} %param.32) | copy-start | bytes 24580
  165.0 5.0 %copy-start.13 = (f32[64]{0:T(128)S(1)}, f32[64]{0:T(128)}, u32[]{:S(2)}) copy-start(f32[64]{0:T(128)} %copy-done.12) | copy-start | bytes 772
where the time goes:
time: 172 us; the launch traced here: 171 us
  waiting for transfers between devices  94.5 us (55%)
  local copies, waits for them, and re-layouts  25.2 us (15%)
  starting transfers between devices  17.6 us (10%)
  matrix products  17.3 us (10%)
  other arithmetic  15.3 us (9%)
    all_to_all x1, waiting for transfers between devices, shards(): lax.all_to_all(outgoing, 'ep', split_axis=1, concat_axis=1, tiled=True)  47.7 us
    all_to_all x1, waiting for transfers between devices, shards(): lax.all_to_all(finished, 'ep', split_axis=1, concat_axis=1, tiled=True)  46.8 us
    all_to_all x1, starting transfers between devices, shards(): lax.all_to_all(send_info, 'ep', split_axis=1, concat_axis=1, tiled=True)  7.33 us
    all_to_all x1, starting transfers between devices, shards(): lax.all_to_all(outgoing, 'ep', split_axis=1, concat_axis=1, tiled=True)  6.14 us
    dot_general x1, matrix products, recurrence(): jnp.dot(merged, w_mix, preferred_element_type=jnp.float32)  5.34 us
    dot_general x1, matrix products, expert_block(): jnp.dot(hidden, w_expert_down[0], preferred_element_type=jnp.float32)  5.3 us
    gather x2, local copies, waits for them, and re-layouts, shards(): jnp.take(gathered.reshape(capacity * experts, model_width), slot_target,...  4.19 us
    all_to_all x1, starting transfers between devices, shards(): lax.all_to_all(finished, 'ep', split_axis=1, concat_axis=1, tiled=True)  4.11 us
  transfers between devices with their start and end apart: 3, of which 2 were waited for; matrix products, arithmetic and copies ran while one was open for 16% of the time, Pallas kernels for 0%

commit v1 on v0

v1 whole, which is shorter than its diff:
```python
import functools

import jax
import jax.numpy as jnp
from jax import lax
from jax.experimental import pallas as pl
from jax.experimental.pallas import tpu as pltpu
from jax.sharding import PartitionSpec as P

epsilon = 1e-06
gate_scale = 8.0
planes = 4
chunks = 4


def rms(values, gain):
    return values * lax.rsqrt(jnp.mean(values * values, axis=-1, keepdims=True) + epsilon) * gain


def mixer_kernel(
    tokens, pre, tap, recur, rate_b, input_b, slope, g_pre, g_post, g_ffn, wb_hbm, wg_hbm, wm_hbm,
    ffn_out, residual_out, branch_out, state_out,
    wb, wg, wm, normed, gate_act, merged, mix, sems,
):
    rows, width = tokens.shape
    channels = pre.shape[1]
    block = rate_b.shape[1]
    loads = [
        pltpu.make_async_copy(src, dst, sems.at[k])
        for k, (src, dst) in enumerate(((wb_hbm, wb), (wg_hbm, wg), (wm_hbm, wm)))
    ]
    for load in loads:
        load.start()
    normed[...] = rms(tokens[...].astype(jnp.float32), g_pre[...]).astype(jnp.bfloat16)
    tile = 256
    loads[0].wait()

    @pl.loop(0, channels // tile)
    def _(t):
        cols = pl.ds(pl.multiple_of(t * tile, tile), tile)
        branch_out[:, cols] = jnp.dot(
            normed[...], wb[:, cols], preferred_element_type=jnp.float32
        ).astype(jnp.bfloat16)

    loads[1].wait()

    @pl.loop(0, channels // tile)
    def _(t):
        cols = pl.ds(pl.multiple_of(t * tile, tile), tile)
        gate_act[:, cols] = jnp.dot(
            normed[...], wg[:, cols], preferred_element_type=jnp.float32
        ).astype(jnp.bfloat16)

    same = lax.broadcasted_iota(jnp.int32, (tile, tile), 0) // block == (
        lax.broadcasted_iota(jnp.int32, (tile, tile), 1) // block
    )

    def spread(ref, t):
        part = ref[pl.ds(t * tile, tile), :].astype(jnp.float32)
        return jnp.where(same, jnp.concatenate([part] * (tile // block), axis=1), 0.0).astype(
            jnp.bfloat16
        )

    for t in range(channels // tile):
        cols = pl.ds(t * tile, tile)
        conv = pre[:, cols] + branch_out[:, cols].astype(jnp.float32) * tap[:, cols]
        conv16 = conv.astype(jnp.bfloat16)
        rate = jax.nn.sigmoid(
            jnp.dot(conv16, spread(rate_b, t), preferred_element_type=jnp.float32)
        )
        inflow = jax.nn.sigmoid(
            jnp.dot(conv16, spread(input_b, t), preferred_element_type=jnp.float32)
        )
        log_decay = rate * slope[:, cols]
        decay = jnp.exp(log_decay)
        rest = -jnp.tanh(log_decay) * (decay * decay + 1.0)
        state = decay * recur[:, cols] + jnp.sqrt(rest) * (inflow * conv)
        state_out[:, cols] = state
        merged[:, cols] = (state * jax.nn.gelu(gate_act[:, cols].astype(jnp.float32))).astype(
            jnp.bfloat16
        )
    loads[2].wait()

    @pl.loop(0, width // tile)
    def _(t):
        cols = pl.ds(pl.multiple_of(t * tile, tile), tile)
        mix[:, cols] = (
            jnp.dot(merged[...], wm[:, cols], preferred_element_type=jnp.float32)
            .astype(jnp.bfloat16)
            .astype(jnp.float32)
        )

    residual = tokens[...].astype(jnp.float32) + rms(mix[...], g_post[...])
    residual_out[...] = residual
    ffn = rms(residual, g_ffn[...]).astype(jnp.bfloat16)
    part = ffn_out.shape[2]
    for c in range(ffn_out.shape[0]):
        ffn_out[c] = ffn[:, c * part : (c + 1) * part]


def experts_kernel(
    n, x, residual, code_rows, code_cols, weight_cols, g_out, wg_hbm, wu_hbm, wd_hbm,
    out,
    wg, wu, wd, xall, sbuf, rbuf, obuf, cbuf, pbuf, fbuf, total,
    load_sem, zs, zr, ds_, dr, os_, orr, ps, pr,
):
    parts, rows, part = x.shape
    group = n // planes
    slab = rbuf.shape[1] // group
    me = lax.axis_index("ep")
    plane, column = me // group, lax.rem(me, group)
    loads = [
        pltpu.make_async_copy(src.at[0], dst, load_sem.at[k])
        for k, (src, dst) in enumerate(((wg_hbm, wg), (wu_hbm, wu), (wd_hbm, wd)))
    ]
    for load in loads:
        load.start()

    def along(d):
        other = lax.rem(plane + d, planes)
        return other, other * group + column

    def beside(d):
        other = lax.rem(column + d, group)
        return other, plane * group + other

    barrier = pltpu.get_barrier_semaphore()
    for d in range(1, planes):
        pl.semaphore_signal(barrier, inc=1, device_id={"ep": along(d)[1]})
    for d in range(1, group):
        pl.semaphore_signal(barrier, inc=1, device_id={"ep": beside(d)[1]})
    pl.semaphore_wait(barrier, planes + group - 2)

    def rcopy(src, dst, send, recv, device):
        return pltpu.make_async_remote_copy(
            src_ref=src, dst_ref=dst, send_sem=send, recv_sem=recv,
            device_id={"ep": device}, device_id_type=pl.DeviceIdType.MESH,
        )

    def strip(k):
        return pl.ds(pl.multiple_of(k * slab, slab), slab)

    def seqs(k):
        return pl.ds(pl.multiple_of(k * rows, rows), rows)

    def token_copy(c, d, landing):
        other, device = along(d)
        spot = other if landing else plane
        return rcopy(
            x.at[c], xall.at[c, seqs(spot)], zs.at[c, other],
            zr.at[c, spot], device,
        )

    def slab_copy(c, d, landing, src, dst, send, recv):
        other, device = beside(d)
        spot = other if landing else column
        return rcopy(
            src.at[c, strip(other)], dst.at[c, strip(spot)], send.at[c, other],
            recv.at[c, spot], device,
        )

    def back_copy(c, d, landing):
        other, device = along(d)
        spot = other if landing else plane
        return rcopy(
            pbuf.at[c, seqs(other)], fbuf.at[c, seqs(spot)], ps.at[c, other],
            pr.at[c, spot], device,
        )

    far = list(range(1, planes))
    near = list(range(1, group))
    for c in range(parts):
        for d in far:
            token_copy(c, d, False).start()
    for c in range(parts):
        xall[c, seqs(plane)] = x[c]

    slots = rbuf.shape[1]
    lots = planes * rows
    row_at = lax.broadcasted_iota(jnp.int32, (slots, lots), 0)
    pick = jnp.zeros((slots, lots), jnp.float32)
    for k in range(code_rows.shape[0]):
        pick = jnp.where(row_at == code_rows[k : k + 1, :], 1.0, pick)
    pick = pick.astype(jnp.bfloat16)

    col_at = lax.broadcasted_iota(jnp.int32, (lots, slots), 1)
    blend = jnp.zeros((lots, slots), jnp.float32)
    for k in range(code_cols.shape[1]):
        blend = jnp.where(col_at == code_cols[:, k : k + 1], weight_cols[:, k : k + 1], blend)
    high = blend.astype(jnp.bfloat16)
    low = (blend - high.astype(jnp.float32)).astype(jnp.bfloat16)

    sums = [None, None]

    def absorb(c):
        for d in near:
            slab_copy(c, d, True, sbuf, rbuf, ds_, dr).wait_recv()
        got = rbuf[c]
        for k, w in enumerate((wg, wu)):
            piece = jnp.dot(
                got, w[c * part : (c + 1) * part, :], preferred_element_type=jnp.float32
            )
            sums[k] = piece if sums[k] is None else sums[k] + piece

    for c in range(parts):
        for d in far:
            token_copy(c, d, True).wait_recv()
        sbuf[c] = jnp.dot(pick, xall[c], preferred_element_type=jnp.float32).astype(jnp.bfloat16)
        for d in near:
            slab_copy(c, d, False, sbuf, rbuf, ds_, dr).start()
        rbuf[c, strip(column)] = sbuf[c, strip(column)]
        if c == 0:
            for load in loads:
                load.wait()
        else:
            absorb(c - 1)
    absorb(parts - 1)
    hidden = (jax.nn.silu(sums[0]) * sums[1]).astype(jnp.bfloat16)

    for c in range(parts):
        obuf[c] = jnp.dot(
            hidden, wd[:, c * part : (c + 1) * part], preferred_element_type=jnp.float32
        ).astype(jnp.bfloat16)
        for d in near:
            slab_copy(c, d, False, obuf, cbuf, os_, orr).start()
        cbuf[c, strip(column)] = obuf[c, strip(column)]

    for c in range(parts):
        for d in near:
            slab_copy(c, d, True, obuf, cbuf, os_, orr).wait_recv()
        got = cbuf[c]
        pbuf[c] = (
            jnp.dot(high, got, preferred_element_type=jnp.float32)
            + jnp.dot(low, got, preferred_element_type=jnp.float32)
        ).astype(jnp.bfloat16)
        for d in far:
            back_copy(c, d, False).start()
        fbuf[c, seqs(plane)] = pbuf[c, seqs(plane)]

    squares = jnp.zeros((rows, 1), jnp.float32)
    for c in range(parts):
        for d in far:
            back_copy(c, d, True).wait_recv()
        summed = fbuf[c, 0:rows].astype(jnp.float32)
        for q in range(1, planes):
            summed = summed + fbuf[c, q * rows : (q + 1) * rows].astype(jnp.float32)
        total[c] = summed
        squares = squares + jnp.sum(summed * summed, axis=1, keepdims=True)
    scale = lax.rsqrt(squares / (parts * part) + epsilon)
    for c in range(parts):
        cols = slice(c * part, (c + 1) * part)
        out[:, cols] = (residual[:, cols] + total[c] * scale * g_out[:, cols]).astype(out.dtype)

    for c in range(parts):
        for d in far:
            token_copy(c, d, False).wait_send()
            back_copy(c, d, False).wait_send()
        for d in near:
            slab_copy(c, d, False, sbuf, rbuf, ds_, dr).wait_send()
            slab_copy(c, d, False, obuf, cbuf, os_, orr).wait_send()


def vmem(count):
    return [pl.BlockSpec(memory_space=pltpu.VMEM)] * count


def anywhere(count):
    return [pl.BlockSpec(memory_space=pl.ANY)] * count


def shards(
    tokens, conv_state, recur_state, w_branch, w_gate, conv_taps, rate_blocks, input_blocks,
    decay_param, w_mix, gain_pre, gain_post, gain_ffn, gain_out, routes, affinity,
    w_expert_gate, w_expert_up, w_expert_down,
):
    n = lax.axis_size("ep")
    me = lax.axis_index("ep")
    rows, width = tokens.shape
    channels = recur_state.shape[1]
    top = routes.shape[1]
    hidden = w_expert_gate.shape[2]
    bf16, f32 = jnp.bfloat16, jnp.float32
    group = n // planes
    capacity = max(2, 3 * rows * top // n)
    limit = rows * top // 2
    slab = -(-planes * capacity // 16) * 16
    slots, lots, part = group * slab, planes * rows, width // chunks

    share = affinity / jnp.sum(affinity, axis=1, keepdims=True)
    info = lax.all_gather(
        jnp.concatenate([routes.astype(f32), share], axis=1), "ep", axis=0, tiled=False
    )
    everyone = info[:, :, :top].astype(jnp.int32).reshape(1, n * rows * top)
    mine = lax.dynamic_index_in_dim(
        info.reshape(planes, group, rows, 2 * top), lax.rem(me, group), 1, keepdims=False
    )
    wanted = mine[:, :, :top].astype(jnp.int32).reshape(planes * rows * top, 1)
    owner = jnp.arange(planes, dtype=jnp.int32) * group + lax.rem(me, group)
    start = jnp.repeat(owner * rows * top, rows * top)[:, None]
    index = start + jnp.tile(jnp.arange(rows * top, dtype=jnp.int32), planes)[:, None]
    place = jnp.arange(n * rows * top, dtype=jnp.int32)[None, :]
    earlier = (everyone == wanted) & (place < index)
    rank = jnp.sum(earlier.astype(jnp.int32), axis=1)
    slot = jnp.sum((earlier & (place >= start)).astype(jnp.int32), axis=1)
    expert = wanted[:, 0] - (me // group) * group
    here = (expert >= 0) & (expert < group)
    source = jnp.repeat(jnp.arange(planes, dtype=jnp.int32), rows * top)
    code = jnp.where(
        here & (rank < limit), expert * slab + source * capacity + slot, -1
    ).reshape(lots, top)
    weight = mine[:, :, top:].reshape(lots, top)

    row = lambda v: v.reshape(1, -1)
    pre = jnp.sum(conv_state.astype(f32) * conv_taps[None, :-1], axis=1)
    slope = row(-gate_scale * jax.nn.softplus(-decay_param))
    block = rate_blocks.shape[1]
    ffn, residual, branch, state_next = pl.pallas_call(
        mixer_kernel,
        out_shape=(
            jax.ShapeDtypeStruct((chunks, rows, part), bf16),
            jax.ShapeDtypeStruct((rows, width), f32),
            jax.ShapeDtypeStruct((rows, channels), bf16),
            jax.ShapeDtypeStruct((rows, channels), f32),
        ),
        in_specs=vmem(10) + anywhere(3),
        out_specs=tuple(vmem(4)),
        scratch_shapes=[
            pltpu.VMEM((width, channels), bf16),
            pltpu.VMEM((width, channels), bf16),
            pltpu.VMEM((channels, width), bf16),
            pltpu.VMEM((rows, width), bf16),
            pltpu.VMEM((rows, channels), bf16),
            pltpu.VMEM((rows, channels), bf16),
            pltpu.VMEM((rows, width), f32),
            pltpu.SemaphoreType.DMA((3,)),
        ],
        compiler_params=pltpu.CompilerParams(vmem_limit_bytes=40 << 20),
    )(
        tokens, pre, conv_taps[-1:], recur_state, rate_blocks.reshape(channels, block),
        input_blocks.reshape(channels, block), slope, row(gain_pre), row(gain_post),
        row(gain_ffn), w_branch, w_gate, w_mix,
    )
    conv_next = jnp.concatenate([conv_state[:, 1:], branch[:, None, :]], axis=1)

    dma = lambda count: pltpu.SemaphoreType.DMA((chunks, count))
    layer_out = pl.pallas_call(
        functools.partial(experts_kernel, n),
        out_shape=jax.ShapeDtypeStruct((rows, width), bf16),
        in_specs=vmem(6) + anywhere(3),
        out_specs=vmem(1)[0],
        scratch_shapes=[
            pltpu.VMEM((width, hidden), bf16),
            pltpu.VMEM((width, hidden), bf16),
            pltpu.VMEM((hidden, width), bf16),
            pltpu.VMEM((chunks, lots, part), bf16),
            pltpu.VMEM((chunks, slots, part), bf16),
            pltpu.VMEM((chunks, slots, part), bf16),
            pltpu.VMEM((chunks, slots, part), bf16),
            pltpu.VMEM((chunks, slots, part), bf16),
            pltpu.VMEM((chunks, lots, part), bf16),
            pltpu.VMEM((chunks, lots, part), bf16),
            pltpu.VMEM((chunks, rows, part), f32),
            pltpu.SemaphoreType.DMA((3,)),
            dma(planes), dma(planes), dma(group), dma(group),
            dma(group), dma(group), dma(planes), dma(planes),
        ],
        compiler_params=pltpu.CompilerParams(
            collective_id=0, has_side_effects=True, vmem_limit_bytes=48 << 20
        ),
    )(
        ffn, residual, code.T, code, weight, row(gain_out),
        w_expert_gate, w_expert_up, w_expert_down,
    )
    return (layer_out, conv_next, state_next)


def solution(mesh):
    ep, copied = "ep", P()
    return jax.shard_map(
        shards,
        mesh=mesh,
        in_specs=(P(ep, None), P(ep, None, None), P(ep, None))
        + (copied,) * 11
        + (P(ep, None),) * 2
        + (P(ep, None, None),) * 3,
        out_specs=(P(ep, None), P(ep, None, None), P(ep, None)),
        check_vma=False,
    )
```

time: 172 us -> 130 us (0.76)
  waiting for transfers between devices: 94.5 us -> 0 us
  Pallas kernels: 0 us -> 70.4 us
  blocking collectives: 0 us -> 43.4 us
  local copies, waits for them, and re-layouts: 25.2 us -> 6.88 us
  starting transfers between devices: 17.6 us -> 0 us
  matrix products: 17.3 us -> 0 us
  other arithmetic: 15.3 us -> 6.76 us
    all_to_all x3 -> x0, waiting for transfers between devices: 94.5 us -> none  [the longest x1 47.7 us: shards(): lax.all_to_all(outgoing, 'ep', split_axis=1, concat_axis=1, tiled=True)]
    pallas_call x0 -> x2, Pallas kernels: none -> 70.4 us  [the longest x1 64.2 us: shards(): pl.pallas_call(functools.partial(experts_kernel, n), out_shape=jax.ShapeD...]
    all_gather x0 -> x1, blocking collectives: none -> 43.4 us  [shards(): lax.all_gather(jnp.concatenate([routes.astype(f32), share], axis=1), 'ep'...]
    all_to_all x3 -> x0, starting transfers between devices: 17.6 us -> none  [the longest x1 7.33 us: shards(): lax.all_to_all(send_info, 'ep', split_axis=1, concat_axis=1, tiled=True)]
    dot_general x6 -> x0, matrix products: 17.3 us -> none  [the longest x1 5.34 us: recurrence(): jnp.dot(merged, w_mix, preferred_element_type=jnp.float32)]
    all_to_all x3 -> x0, local copies, waits for them, and re-layouts: 6.9 us -> none  [the longest x1 3.61 us: shards(): lax.all_to_all(finished, 'ep', split_axis=1, concat_axis=1, tiled=True)]
    reshape x4 -> x0, local copies, waits for them, and re-layouts: 5.5 us -> none  [the longest x1 3.66 us: shards(): outgoing = outgoing.reshape(capacity, experts, model_width)]
    gather x2 -> x0, local copies, waits for them, and re-layouts: 4.19 us -> none  [shards(): jnp.take(gathered.reshape(capacity * experts, model_width), slot_target,...]
  transfers between devices with their start and end apart: 3 -> 0, of which waited for: 2 -> 0; matrix products, arithmetic and copies ran while one was open for 16% -> 0% of each run, Pallas kernels for 0% -> 0%
where the time goes in v1:
time: 130 us; the launch traced here: 128 us
  Pallas kernels  70.4 us (54%)
  blocking collectives  43.4 us (33%)
  local copies, waits for them, and re-layouts  6.88 us (5%)
  other arithmetic  6.76 us (5%)
    pallas_call x1, Pallas kernels, shards(): pl.pallas_call(functools.partial(experts_kernel, n), out_shape=jax.ShapeD...  64.2 us
    all_gather x1, blocking collectives, shards(): lax.all_gather(jnp.concatenate([routes.astype(f32), share], axis=1), 'ep'...  43.4 us
    pallas_call x1, Pallas kernels, shards(): pl.pallas_call(mixer_kernel, out_shape=(jax.ShapeDtypeStruct((chunks, row...  6.19 us
    unnamed x31, local copies, waits for them, and re-layouts  5.13 us
    reduce_sum x1, other arithmetic, shards(): rank = jnp.sum(earlier.astype(jnp.int32), axis=1)  3.39 us

profile of v1, /device:TPU:0, one launch (start us, length us, event | category | flops | bytes accessed | tf_op | source)
XLA Modules:
  0.0 128.4 jit_solution(7936037213949016134)
XLA Ops:
  0.6 0.0 copy-start.13
  0.6 0.0 copy-start.12
  0.7 0.0 copy-start.14
  0.7 0.0 copy-start.6
  0.7 0.0 copy-start.7
  0.7 0.0 copy-start.9
  0.7 0.0 copy-start.10
  0.7 0.0 copy-start.11
  0.7 0.0 copy-start.4
  0.7 0.0 copy-start.5
  0.7 0.8 reduce_sum.39
  1.5 0.7 broadcast_divide_fusion
  2.2 0.7 convert_element_type.19
  2.9 43.4 %all-gather.1 = f32[32,64,4]{1,2,0:T(4,128)S(1)} all-gather(f32[1,64,4]{1,2,0:T(4,128)S(1)} %maximum_bitcast_fusion), channel_id=2, replica_groups=mesh['ep'=32] {'ep'}, dimensions={0}, use_global_device_ids=true | all-gather | bytes 33792 | tf_op jit(solution)/shard_map/all_gather | solution.py:290
  46.3 0.1 copy.33
  46.5 0.1 fusion.5
  46.6 0.1 eq.19
  46.7 0.1 bitcast_add_fusion.1
  46.8 0.1 broadcast_bitcast_fusion
  46.9 0.4 copy.35
  47.3 0.5 eq.17
  47.8 3.4 %convert_reduce_fusion.1 = (s32[512]{0:T(512)S(1)}, s32[512]{0:T(512)S(1)}) fusion(s32[512]{0:T(512)S(1)} %bitcast_add_fusion.1, s32[4096]{0:T(1024)S(1)} %eq.17, s32[512]{0:T(512)S(1)} %eq.19, s32[512]{0:T(512)S(1)} %broadcast_bitcast_fusion), kind=kLoop, calls=%fused_computation.2 | loop fusion | flops 18873344 | bytes 26624 | tf_op jit(solution)/shard_map/reduce_sum | solution.py:303
  51.2 0.1 reduce_sum.42
  51.3 0.2 lt.45
  51.6 0.1 mul.59
  51.8 0.1 copy.36.code_rows
  51.9 0.0 copy-done.13
  51.9 0.0 copy-done.12
  51.9 0.1 multiply_reduce_fusion.pre
  52.0 0.0 copy-done.14
  52.0 0.0 copy-done.6
  52.0 0.0 copy-done.7
  52.1 0.0 copy-done.9
  52.1 0.0 copy-done.10
  52.1 0.0 copy-done.11
  52.1 0.0 copy-done.4
  52.1 0.0 copy-done.5
  52.1 0.0 copy-start
  52.1 2.2 %copy-done = bf16[2048,1024]{1,0:T(8,128)(2,1)S(1)} copy-done((bf16[2048,1024]{1,0:T(8,128)(2,1)S(1)}, bf16[2048,1024]{1,0:T(8,128)(2,1)}, u32[]{:S(2)}) %copy-start) | copy-done | bytes 4194328
  54.3 0.0 copy-start.1
  54.3 2.2 %copy-done.1 = bf16[2048,1024]{1,0:T(8,128)(2,1)S(1)} copy-done((bf16[2048,1024]{1,0:T(8,128)(2,1)S(1)}, bf16[2048,1024]{1,0:T(8,128)(2,1)}, u32[]{:S(2)}) %copy-start.1) | copy-done | bytes 4194328
  56.5 0.0 copy-start.2
  56.5 0.0 copy-start.3
  56.5 0.0 copy-start.8
  56.5 6.2 %shard_map.202 = (bf16[4,64,512]{2,1,0:T(8,128)(2,1)S(1)}, f32[64,2048]{1,0:T(8,128)S(1)}, bf16[64,1024]{1,0:T(8,128)(2,1)S(1)}, f32[64,1024]{1,0:T(8,128)}) custom-call(bf16[64,2048]{1,0:T(8,128)(2,1)S(1)} %copy-done.4, f32[64,1024]{1,0:T(8,128)S(1)} %multiply_reduce_fusion.pre, f32[1,1024]{1,0:T(1,128)S(1)} %slice.19.tap, f32[64,1024]{1,0:T(8,128)S(1)} %copy-done.5, ...), custom_call_target="tpu_custom_call" | custom-call | tf_op jit(solution)/shard_map/pallas_call | solution.py:317
  62.7 0.0 slice-start
  62.7 0.0 copy-done.2
  62.7 0.0 copy-done.3
  62.7 0.0 copy-done.8
  62.7 64.2 %shard_map.203 = bf16[64,2048]{1,0:T(8,128)(2,1)S(1)} custom-call(bf16[4,64,512]{2,1,0:T(8,128)(2,1)S(1)} %get-tuple-element.7.x, f32[64,2048]{1,0:T(8,128)S(1)} %get-tuple-element.8.residual, s32[2,256]{1,0:T(2,128)S(1)} %copy.36.code_rows, s32[256,2]{1,0:T(8,128)S(1)} %fusion.3.code_cols, f32[256,2]{1,0:T(8,128)S(1)} %bitcast.31, f32[1,2048]{1,0:T(1,128)S(1)} %bitcast.36, ...), custom_call_target="tpu_custom_call" | custom-call | tf_op jit(solution)/shard_map/pallas_call | solution.py:346
  126.9 0.0 slice-done
  126.9 0.8 pad_maximum_fusion
  127.7 0.7 copy.40
  (12 shorter events, 0.2 us)
Async XLA Ops:
  0.6 51.3 %copy-start.13 = (f32[4,1024]{1,0:T(4,128)S(1)}, f32[4,1024]{1,0:T(4,128)}, u32[]{:S(2)}) copy-start(f32[4,1024]{1,0:T(4,128)} %param.24) | copy-start | bytes 49156
  0.6 51.2 %copy-start.12 = (bf16[64,3,1024]{2,0,1:T(8,128)(2,1)S(1)}, bf16[64,3,1024]{2,0,1:T(8,128)(2,1)}, u32[]{:S(2)}) copy-start(bf16[64,3,1024]{2,0,1:T(8,128)(2,1)} %param.20) | copy-start | bytes 1179652
  0.7 51.3 %copy-start.14 = (f32[1024]{0:T(1024)S(1)}, f32[1024]{0:T(1024)}, u32[]{:S(2)}) copy-start(f32[1024]{0:T(1024)} %param.27) | copy-start | bytes 12292
  0.7 51.4 %copy-start.6 = (bf16[16,64,64]{2,1,0:T(8,128)(2,1)S(1)}, bf16[16,64,64]{2,1,0:T(8,128)(2,1)}, u32[]{:S(2)}) copy-start(bf16[16,64,64]{2,1,0:T(8,128)(2,1)} %param.25) | copy-start | bytes 393220
  0.7 51.4 %copy-start.7 = (bf16[16,64,64]{2,1,0:T(8,128)(2,1)S(1)}, bf16[16,64,64]{2,1,0:T(8,128)(2,1)}, u32[]{:S(2)}) copy-start(bf16[16,64,64]{2,1,0:T(8,128)(2,1)} %param.26) | copy-start | bytes 393220
  0.7 51.4 %copy-start.9 = (f32[2048]{0:T(1024)S(1)}, f32[2048]{0:T(1024)}, u32[]{:S(2)}) copy-start(f32[2048]{0:T(1024)} %param.29) | copy-start | bytes 24580
  0.7 51.4 %copy-start.10 = (f32[2048]{0:T(1024)S(1)}, f32[2048]{0:T(1024)}, u32[]{:S(2)}) copy-start(f32[2048]{0:T(1024)} %param.30) | copy-start | bytes 24580
  0.7 51.4 %copy-start.11 = (f32[2048]{0:T(1024)S(1)}, f32[2048]{0:T(1024)}, u32[]{:S(2)}) copy-start(f32[2048]{0:T(1024)} %param.31) | copy-start | bytes 24580
  0.7 51.4 %copy-start.4 = (bf16[64,2048]{1,0:T(8,128)(2,1)S(1)}, bf16[64,2048]{1,0:T(8,128)(2,1)}, u32[]{:S(2)}) copy-start(bf16[64,2048]{1,0:T(8,128)(2,1)} %tokens.1) | copy-start | bytes 786436
  0.7 51.4 %copy-start.5 = (f32[64,1024]{1,0:T(8,128)S(1)}, f32[64,1024]{1,0:T(8,128)}, u32[]{:S(2)}) copy-start(f32[64,1024]{1,0:T(8,128)} %recur.1) | copy-start | bytes 786436
  52.1 2.2 %copy-start = (bf16[2048,1024]{1,0:T(8,128)(2,1)S(1)}, bf16[2048,1024]{1,0:T(8,128)(2,1)}, u32[]{:S(2)}) copy-start(bf16[2048,1024]{1,0:T(8,128)(2,1)} %wb_hbm.1) | copy-start | bytes 12582916
  54.3 2.2 %copy-start.1 = (bf16[2048,1024]{1,0:T(8,128)(2,1)S(1)}, bf16[2048,1024]{1,0:T(8,128)(2,1)}, u32[]{:S(2)}) copy-start(bf16[2048,1024]{1,0:T(8,128)(2,1)} %wg_hbm.2) | copy-start | bytes 12582916
  56.5 6.2 %copy-start.2 = (bf16[1,2048,512]{2,1,0:T(8,128)(2,1)S(1)}, bf16[1,2048,512]{2,1,0:T(8,128)(2,1)}, u32[]{:S(2)}) copy-start(bf16[1,2048,512]{2,1,0:T(8,128)(2,1)} %wg_hbm.3) | copy-start | bytes 6291460
  56.5 6.2 %copy-start.3 = (bf16[1,2048,512]{2,1,0:T(8,128)(2,1)S(1)}, bf16[1,2048,512]{2,1,0:T(8,128)(2,1)}, u32[]{:S(2)}) copy-start(bf16[1,2048,512]{2,1,0:T(8,128)(2,1)} %wu_hbm.1) | copy-start | bytes 6291460
  56.5 6.2 %copy-start.8 = (f32[2048]{0:T(1024)S(1)}, f32[2048]{0:T(1024)}, u32[]{:S(2)}) copy-start(f32[2048]{0:T(1024)} %param.32) | copy-start | bytes 24580
  62.7 64.2 %slice-start = ((bf16[64,3,1024]{2,0,1:T(8,128)(2,1)}), bf16[64,2,1024]{2,0,1:T(8,128)(2,1)S(1)}, s32[]{:S(2)}) async-start(bf16[64,3,1024]{2,0,1:T(8,128)(2,1)} %param.20), calls=%async_computation | async-start | bytes 524288 | tf_op jit(solution)/shard_map/slice | solution.py:343

commit v2 on v1

--- a/solution.py
+++ b/solution.py
@@ -17,20 +17,42 @@
     return values * lax.rsqrt(jnp.mean(values * values, axis=-1, keepdims=True) + epsilon) * gain
 
 
-def mixer_kernel(
-    tokens, pre, tap, recur, rate_b, input_b, slope, g_pre, g_post, g_ffn, wb_hbm, wg_hbm, wm_hbm,
-    ffn_out, residual_out, branch_out, state_out,
-    wb, wg, wm, normed, gate_act, merged, mix, sems,
+def layer_kernel(
+    n, capacity, limit, top,
+    tokens, pre, tap, recur, rate_b, input_b, slope, g_pre, g_post, g_ffn, g_out, message,
+    wb_hbm, wg_hbm, wm_hbm, eg_hbm, eu_hbm, ed_hbm,
+    out, branch_out, state_out,
+    wb, wg, wm, normed, gate_act, merged, mix, residual, mall,
+    eg, eu, ed, xall, sbuf, rbuf, obuf, cbuf, pbuf, fbuf, total,
+    load_sem, ms, mr, zs, zr, ds_, dr, os_, orr, ps, pr,
 ):
+    parts, lots, part = xall.shape
+    group = n // planes
+    slots = rbuf.shape[1]
+    slab = slots // group
+    me = lax.axis_index("ep")
+    plane, column = me // group, lax.rem(me, group)
     rows, width = tokens.shape
     channels = pre.shape[1]
     block = rate_b.shape[1]
     loads = [
-        pltpu.make_async_copy(src, dst, sems.at[k])
-        for k, (src, dst) in enumerate(((wb_hbm, wb), (wg_hbm, wg), (wm_hbm, wm)))
+        pltpu.make_async_copy(src, dst, load_sem.at[k])
+        for k, (src, dst) in enumerate(
+            (
+                (wb_hbm, wb), (wg_hbm, wg), (wm_hbm, wm),
+                (eg_hbm.at[0], eg), (eu_hbm.at[0], eu), (ed_hbm.at[0], ed),
+            )
+        )
     ]
     for load in loads:
         load.start()
+
+    barrier = pltpu.get_barrier_semaphore()
+
+    @pl.loop(1, n)
+    def _(d):
+        pl.semaphore_signal(barrier, inc=1, device_id={"ep": lax.rem(me + d, n)})
+
     normed[...] = rms(tokens[...].astype(jnp.float32), g_pre[...]).astype(jnp.bfloat16)
     tile = 256
     loads[0].wait()
@@ -42,6 +64,25 @@
             normed[...], wb[:, cols], preferred_element_type=jnp.float32
         ).astype(jnp.bfloat16)
 
+    def lanes(k):
+        return pl.ds(pl.multiple_of(k * message.shape[1], message.shape[1]), message.shape[1])
+
+    def message_copy(d, landing):
+        device = lax.rem(me + d, n)
+        spot = device if landing else me
+        return pltpu.make_async_remote_copy(
+            src_ref=message, dst_ref=mall.at[:, lanes(spot)], send_sem=ms.at[device],
+            recv_sem=mr.at[spot], device_id={"ep": device},
+            device_id_type=pl.DeviceIdType.MESH,
+        )
+
+    pl.semaphore_wait(barrier, n - 1)
+
+    @pl.loop(1, n)
+    def _(d):
+        message_copy(d, False).start()
+
+    mall[:, lanes(me)] = message[...]
     loads[1].wait()
 
     @pl.loop(0, channels // tile)
@@ -90,31 +131,11 @@
             .astype(jnp.float32)
         )
 
-    residual = tokens[...].astype(jnp.float32) + rms(mix[...], g_post[...])
-    residual_out[...] = residual
-    ffn = rms(residual, g_ffn[...]).astype(jnp.bfloat16)
-    part = ffn_out.shape[2]
-    for c in range(ffn_out.shape[0]):
-        ffn_out[c] = ffn[:, c * part : (c + 1) * part]
-
-
-def experts_kernel(
-    n, x, residual, code_rows, code_cols, weight_cols, g_out, wg_hbm, wu_hbm, wd_hbm,
-    out,
-    wg, wu, wd, xall, sbuf, rbuf, obuf, cbuf, pbuf, fbuf, total,
-    load_sem, zs, zr, ds_, dr, os_, orr, ps, pr,
-):
-    parts, rows, part = x.shape
-    group = n // planes
-    slab = rbuf.shape[1] // group
-    me = lax.axis_index("ep")
-    plane, column = me // group, lax.rem(me, group)
-    loads = [
-        pltpu.make_async_copy(src.at[0], dst, load_sem.at[k])
-        for k, (src, dst) in enumerate(((wg_hbm, wg), (wu_hbm, wu), (wd_hbm, wd)))
-    ]
-    for load in loads:
-        load.start()
+    residual[...] = tokens[...].astype(jnp.float32) + rms(mix[...], g_post[...])
+    ffn = rms(residual[...], g_ffn[...]).astype(jnp.bfloat16)
+    own = pl.ds(pl.multiple_of(plane * rows, rows), rows)
+    for c in range(parts):
+        xall[c, own] = ffn[:, c * part : (c + 1) * part]
 
     def along(d):
         other = lax.rem(plane + d, planes)
@@ -123,13 +144,6 @@
     def beside(d):
         other = lax.rem(column + d, group)
         return other, plane * group + other
-
-    barrier = pltpu.get_barrier_semaphore()
-    for d in range(1, planes):
-        pl.semaphore_signal(barrier, inc=1, device_id={"ep": along(d)[1]})
-    for d in range(1, group):
-        pl.semaphore_signal(barrier, inc=1, device_id={"ep": beside(d)[1]})
-    pl.semaphore_wait(barrier, planes + group - 2)
 
     def rcopy(src, dst, send, recv, device):
         return pltpu.make_async_remote_copy(
@@ -147,7 +161,7 @@
         other, device = along(d)
         spot = other if landing else plane
         return rcopy(
-            x.at[c], xall.at[c, seqs(spot)], zs.at[c, other],
+            xall.at[c, seqs(plane)], xall.at[c, seqs(spot)], zs.at[c, other],
             zr.at[c, spot], device,
         )
 
@@ -172,23 +186,58 @@
     for c in range(parts):
         for d in far:
             token_copy(c, d, False).start()
-    for c in range(parts):
-        xall[c, seqs(plane)] = x[c]
-
-    slots = rbuf.shape[1]
-    lots = planes * rows
-    row_at = lax.broadcasted_iota(jnp.int32, (slots, lots), 0)
-    pick = jnp.zeros((slots, lots), jnp.float32)
-    for k in range(code_rows.shape[0]):
-        pick = jnp.where(row_at == code_rows[k : k + 1, :], 1.0, pick)
+
+    @pl.loop(1, n)
+    def _(d):
+        message_copy(d, True).wait_recv()
+
+    f32 = jnp.float32
+    names = lax.broadcasted_iota(jnp.int32, (group, 1), 0)
+    named = (names + plane * group).astype(f32)
+    every = jnp.zeros((group, mall.shape[1]), f32)
+    for k in range(top):
+        every = every + jnp.where(mall[k : k + 1, :] == named, 1.0, 0.0)
+    device_at = lax.broadcasted_iota(jnp.int32, every.shape, 1) // message.shape[1]
+    lot_at = lax.broadcasted_iota(jnp.int32, (1, lots), 1)
+    base = jnp.zeros((group, lots), f32)
+    current = []
+    for q in range(planes):
+        device = q * group + column
+        before = jnp.sum(jnp.where(device_at < device, every, 0.0), axis=1, keepdims=True)
+        base = jnp.where(lot_at // rows == q, before, base)
+        current.append(mall[:, lanes(device)][:, :rows])
+    current = jnp.concatenate(current, axis=1)
+    one = [jnp.where(current[k : k + 1, :] == named, 1.0, 0.0) for k in range(top)]
+    left = lax.broadcasted_iota(jnp.int32, (lots, lots), 0)
+    right = lax.broadcasted_iota(jnp.int32, (lots, lots), 1)
+    upper = jnp.where((left // rows == right // rows) & (left < right), 1.0, 0.0)
+    slot = jnp.dot(
+        sum(one).astype(jnp.bfloat16), upper.astype(jnp.bfloat16), preferred_element_type=f32
+    )
+    spot_of = jnp.where(
+        base + slot < limit,
+        (names * slab + (lot_at // rows) * capacity + 1).astype(f32) + slot,
+        0.0,
+    )
+    codes = [jnp.sum(one[k] * spot_of, axis=0, keepdims=True) - 1.0 for k in range(top)]
+    raw = [current[top + k : top + k + 1, :] for k in range(top)]
+    shares = [r / sum(raw) for r in raw]
+    spare = [jnp.zeros((1, lots), f32)] * (-2 * top % 8)
+    turned = jnp.transpose(jnp.concatenate(codes + shares + spare, axis=0))
+
+    row_at = lax.broadcasted_iota(jnp.int32, (slots, lots), 0).astype(f32)
+    pick = jnp.zeros((slots, lots), f32)
+    for k in range(top):
+        pick = jnp.where(row_at == codes[k], 1.0, pick)
     pick = pick.astype(jnp.bfloat16)
-
-    col_at = lax.broadcasted_iota(jnp.int32, (lots, slots), 1)
-    blend = jnp.zeros((lots, slots), jnp.float32)
-    for k in range(code_cols.shape[1]):
-        blend = jnp.where(col_at == code_cols[:, k : k + 1], weight_cols[:, k : k + 1], blend)
+    col_at = lax.broadcasted_iota(jnp.int32, (lots, slots), 1).astype(f32)
+    blend = jnp.zeros((lots, slots), f32)
+    for k in range(top):
+        blend = jnp.where(
+            col_at == turned[:, k : k + 1], turned[:, top + k : top + k + 1], blend
+        )
     high = blend.astype(jnp.bfloat16)
-    low = (blend - high.astype(jnp.float32)).astype(jnp.bfloat16)
+    low = (blend - high.astype(f32)).astype(jnp.bfloat16)
 
     sums = [None, None]
 
@@ -196,7 +245,7 @@
         for d in near:
             slab_copy(c, d, True, sbuf, rbuf, ds_, dr).wait_recv()
         got = rbuf[c]
-        for k, w in enumerate((wg, wu)):
+        for k, w in enumerate((eg, eu)):
             piece = jnp.dot(
                 got, w[c * part : (c + 1) * part, :], preferred_element_type=jnp.float32
             )
@@ -210,7 +259,7 @@
             slab_copy(c, d, False, sbuf, rbuf, ds_, dr).start()
         rbuf[c, strip(column)] = sbuf[c, strip(column)]
         if c == 0:
-            for load in loads:
+            for load in loads[3:]:
                 load.wait()
         else:
             absorb(c - 1)
@@ -219,7 +268,7 @@
 
     for c in range(parts):
         obuf[c] = jnp.dot(
-            hidden, wd[:, c * part : (c + 1) * part], preferred_element_type=jnp.float32
+            hidden, ed[:, c * part : (c + 1) * part], preferred_element_type=jnp.float32
         ).astype(jnp.bfloat16)
         for d in near:
             slab_copy(c, d, False, obuf, cbuf, os_, orr).start()
@@ -251,6 +300,10 @@
         cols = slice(c * part, (c + 1) * part)
         out[:, cols] = (residual[:, cols] + total[c] * scale * g_out[:, cols]).astype(out.dtype)
 
+    @pl.loop(1, n)
+    def _(d):
+        message_copy(d, False).wait_send()
+
     for c in range(parts):
         for d in far:
             token_copy(c, d, False).wait_send()
@@ -274,7 +327,6 @@
     w_expert_gate, w_expert_up, w_expert_down,
 ):
     n = lax.axis_size("ep")
-    me = lax.axis_index("ep")
     rows, width = tokens.shape
     channels = recur_state.shape[1]
     top = routes.shape[1]
@@ -286,44 +338,25 @@
     slab = -(-planes * capacity // 16) * 16
     slots, lots, part = group * slab, planes * rows, width // chunks
 
-    share = affinity / jnp.sum(affinity, axis=1, keepdims=True)
-    info = lax.all_gather(
-        jnp.concatenate([routes.astype(f32), share], axis=1), "ep", axis=0, tiled=False
-    )
-    everyone = info[:, :, :top].astype(jnp.int32).reshape(1, n * rows * top)
-    mine = lax.dynamic_index_in_dim(
-        info.reshape(planes, group, rows, 2 * top), lax.rem(me, group), 1, keepdims=False
-    )
-    wanted = mine[:, :, :top].astype(jnp.int32).reshape(planes * rows * top, 1)
-    owner = jnp.arange(planes, dtype=jnp.int32) * group + lax.rem(me, group)
-    start = jnp.repeat(owner * rows * top, rows * top)[:, None]
-    index = start + jnp.tile(jnp.arange(rows * top, dtype=jnp.int32), planes)[:, None]
-    place = jnp.arange(n * rows * top, dtype=jnp.int32)[None, :]
-    earlier = (everyone == wanted) & (place < index)
-    rank = jnp.sum(earlier.astype(jnp.int32), axis=1)
-    slot = jnp.sum((earlier & (place >= start)).astype(jnp.int32), axis=1)
-    expert = wanted[:, 0] - (me // group) * group
-    here = (expert >= 0) & (expert < group)
-    source = jnp.repeat(jnp.arange(planes, dtype=jnp.int32), rows * top)
-    code = jnp.where(
-        here & (rank < limit), expert * slab + source * capacity + slot, -1
-    ).reshape(lots, top)
-    weight = mine[:, :, top:].reshape(lots, top)
+    message = jnp.concatenate([routes.T.astype(f32), affinity.T], axis=0)
+    message = jnp.pad(
+        message, ((0, -2 * top % 8), (0, -rows % 128)), constant_values=-1.0
+    )
 
     row = lambda v: v.reshape(1, -1)
     pre = jnp.sum(conv_state.astype(f32) * conv_taps[None, :-1], axis=1)
     slope = row(-gate_scale * jax.nn.softplus(-decay_param))
     block = rate_blocks.shape[1]
-    ffn, residual, branch, state_next = pl.pallas_call(
-        mixer_kernel,
+    dma = lambda *count: pltpu.SemaphoreType.DMA(count)
+    layer_out, branch, state_next = pl.pallas_call(
+        functools.partial(layer_kernel, n, capacity, limit, top),
         out_shape=(
-            jax.ShapeDtypeStruct((chunks, rows, part), bf16),
-            jax.ShapeDtypeStruct((rows, width), f32),
+            jax.ShapeDtypeStruct((rows, width), bf16),
             jax.ShapeDtypeStruct((rows, channels), bf16),
             jax.ShapeDtypeStruct((rows, channels), f32),
         ),
-        in_specs=vmem(10) + anywhere(3),
-        out_specs=tuple(vmem(4)),
+        in_specs=vmem(12) + anywhere(6),
+        out_specs=tuple(vmem(3)),
         scratch_shapes=[
             pltpu.VMEM((width, channels), bf16),
             pltpu.VMEM((width, channels), bf16),
@@ -332,23 +365,8 @@
             pltpu.VMEM((rows, channels), bf16),
             pltpu.VMEM((rows, channels), bf16),
             pltpu.VMEM((rows, width), f32),
-            pltpu.SemaphoreType.DMA((3,)),
-        ],
-        compiler_params=pltpu.CompilerParams(vmem_limit_bytes=40 << 20),
-    )(
-        tokens, pre, conv_taps[-1:], recur_state, rate_blocks.reshape(channels, block),
-        input_blocks.reshape(channels, block), slope, row(gain_pre), row(gain_post),
-        row(gain_ffn), w_branch, w_gate, w_mix,
-    )
-    conv_next = jnp.concatenate([conv_state[:, 1:], branch[:, None, :]], axis=1)
-
-    dma = lambda count: pltpu.SemaphoreType.DMA((chunks, count))
-    layer_out = pl.pallas_call(
-        functools.partial(experts_kernel, n),
-        out_shape=jax.ShapeDtypeStruct((rows, width), bf16),
-        in_specs=vmem(6) + anywhere(3),
-        out_specs=vmem(1)[0],
-        scratch_shapes=[
+            pltpu.VMEM((rows, width), f32),
+            pltpu.VMEM((message.shape[0], n * message.shape[1]), f32),
             pltpu.VMEM((width, hidden), bf16),
             pltpu.VMEM((width, hidden), bf16),
             pltpu.VMEM((hidden, width), bf16),
@@ -360,17 +378,20 @@
             pltpu.VMEM((chunks, lots, part), bf16),
             pltpu.VMEM((chunks, lots, part), bf16),
             pltpu.VMEM((chunks, rows, part), f32),
-            pltpu.SemaphoreType.DMA((3,)),
-            dma(planes), dma(planes), dma(group), dma(group),
-            dma(group), dma(group), dma(planes), dma(planes),
+            dma(6), dma(n), dma(n),
+            dma(chunks, planes), dma(chunks, planes), dma(chunks, group), dma(chunks, group),
+            dma(chunks, group), dma(chunks, group), dma(chunks, planes), dma(chunks, planes),
         ],
         compiler_params=pltpu.CompilerParams(
-            collective_id=0, has_side_effects=True, vmem_limit_bytes=48 << 20
+            collective_id=0, has_side_effects=True, vmem_limit_bytes=60 << 20
         ),
     )(
-        ffn, residual, code.T, code, weight, row(gain_out),
-        w_expert_gate, w_expert_up, w_expert_down,
-    )
+        tokens, pre, conv_taps[-1:], recur_state, rate_blocks.reshape(channels, block),
+        input_blocks.reshape(channels, block), slope, row(gain_pre), row(gain_post),
+        row(gain_ffn), row(gain_out), message,
+        w_branch, w_gate, w_mix, w_expert_gate, w_expert_up, w_expert_down,
+    )
+    conv_next = jnp.concatenate([conv_state[:, 1:], branch[:, None, :]], axis=1)
     return (layer_out, conv_next, state_next)
 
 

time: 130 us -> 90.4 us (0.70)
  blocking collectives: 43.4 us -> 0 us
  Pallas kernels: 70.4 us -> 77.5 us
  local copies, waits for them, and re-layouts: 6.88 us -> 4.66 us
    all_gather x1 -> x0, blocking collectives: 43.4 us -> none  [shards(): lax.all_gather(jnp.concatenate([routes.astype(f32), share], axis=1), 'ep'...]
    pallas_call x2 -> x1, Pallas kernels: 70.4 us -> 77.5 us  [shards(): pl.pallas_call(functools.partial(layer_kernel, n, capacity, limit, top),...]
    reduce_sum x2 -> x0, other arithmetic: 4.18 us -> none  [the longest x1 3.39 us: shards(): rank = jnp.sum(earlier.astype(jnp.int32), axis=1)]
    unnamed x31 -> x2, local copies, waits for them, and re-layouts: 5.13 us -> 3.34 us
    reduce_sum x1, other arithmetic: 0.1 us -> 1.8 us  [shards(): pre = jnp.sum(conv_state.astype(f32) * conv_taps[None, :-1], axis=1)]
    slice x1, local copies, waits for them, and re-layouts: 0.01 us -> 1.31 us  [shards(): conv_taps[-1:]]
where the time goes in v2:
time: 90.4 us; the launch traced here: 89.6 us
  Pallas kernels  77.5 us (86%)
  other arithmetic  6.75 us (7%)
  local copies, waits for them, and re-layouts  4.66 us (5%)
    pallas_call x1, Pallas kernels, shards(): pl.pallas_call(functools.partial(layer_kernel, n, capacity, limit, top),...  77.5 us
    unnamed x2, local copies, waits for them, and re-layouts  3.34 us

profile of v2, /device:TPU:0, one launch (start us, length us, event | category | flops | bytes accessed | tf_op | source)
XLA Modules:
  0.0 89.6 jit_solution(9632688750940579811)
XLA Ops:
  0.6 0.7 convert_bitcast_fusion
  1.3 1.3 %select_maximum_fusion.message = f32[8,128]{1,0:T(8,128)} fusion(f32[2,64]{1,0:T(2,128)} %bitcast.21, f32[2,64]{1,0:T(2,128)S(1)} %convert_bitcast_fusion), kind=kLoop, calls=%fused_computation.4 | loop fusion | flops 8192 | bytes 5120 | tf_op jit(solution)/shard_map/concatenate | solution.py:341
  2.6 1.3 %fusion = f32[1024]{0:T(1024)} fusion(f32[1024]{0:T(1024)} %param.27), kind=kLoop, calls=%fused_computation.3 | loop fusion | flops 8192 | bytes 8192 | tf_op jit(solution)/shard_map/mul | solution.py:348
  3.9 1.3 %slice.10.tap = f32[1,1024]{1,0:T(1,128)} slice(f32[4,1024]{1,0:T(4,128)} %param.24), slice={[3:4], [0:1024]} | slice | bytes 8192 | tf_op jit(solution)/shard_map/slice | solution.py:389
  5.2 1.8 %multiply_reduce_fusion.pre = f32[64,1024]{1,0:T(8,128)} fusion(bf16[64,3,1024]{2,0,1:T(8,128)(2,1)} %param.20, f32[3,1024]{1,0:T(4,128)} %bitcast.15), kind=kLoop, calls=%fused_computation | loop fusion | flops 524288 | bytes 667648 | tf_op jit(solution)/shard_map/reduce_sum | solution.py:347
  7.0 0.0 slice-start
  7.0 77.5 %shard_map.202 = (bf16[64,2048]{1,0:T(8,128)(2,1)}, bf16[64,1024]{1,0:T(8,128)(2,1)}, f32[64,1024]{1,0:T(8,128)}) custom-call(bf16[64,2048]{1,0:T(8,128)(2,1)} %tokens.1, f32[64,1024]{1,0:T(8,128)} %multiply_reduce_fusion.pre, f32[1,1024]{1,0:T(1,128)} %slice.10.tap, f32[64,1024]{1,0:T(8,128)} %recur.1, bf16[1024,64]{1,0:T(8,128)(2,1)} %bitcast.12, ...), custom_call_target="tpu_custom_call" | custom-call | tf_op jit(solution)/shard_map/pallas_call | solution.py:351
  84.6 0.0 slice-done
  84.6 1.7 %pad_maximum_fusion = bf16[64,3,1024]{2,0,1:T(8,128)(2,1)} fusion(bf16[64,1,1024]{2,0,1:T(8,128)(2,1)} %bitcast.14, bf16[64,2,1024]{2,0,1:T(8,128)(2,1)S(1)} %slice-done), kind=kLoop, calls=%fused_computation.1 | loop fusion | flops 196608 | bytes 786432 | tf_op jit(solution)/shard_map/concatenate | solution.py:394
  86.3 1.7 %copy.24 = bf16[64,2048]{1,0:T(8,128)(2,1)} copy(bf16[64,2048]{1,0:T(8,128)(2,1)} %get-tuple-element.12) | data formatting | bytes 524288
  87.9 1.7 %copy.25 = f32[64,1024]{1,0:T(8,128)} copy(f32[64,1024]{1,0:T(8,128)} %get-tuple-element.14) | data formatting | bytes 524288
Async XLA Ops:
  7.0 77.6 %slice-start = ((bf16[64,3,1024]{2,0,1:T(8,128)(2,1)}), bf16[64,2,1024]{2,0,1:T(8,128)(2,1)S(1)}, s32[]{:S(2)}) async-start(bf16[64,3,1024]{2,0,1:T(8,128)(2,1)} %param.20), calls=%async_computation | async-start | bytes 524288 | tf_op jit(solution)/shard_map/slice | solution.py:394

commit v3 on v2

--- a/solution.py
+++ b/solution.py
@@ -19,10 +19,10 @@
 
 def layer_kernel(
     n, capacity, limit, top,
-    tokens, pre, tap, recur, rate_b, input_b, slope, g_pre, g_post, g_ffn, g_out, message,
+    tokens, pre, taps, recur, rate_b, input_b, decay_p, g_pre, g_post, g_ffn, g_out, routes, affinity,
     wb_hbm, wg_hbm, wm_hbm, eg_hbm, eu_hbm, ed_hbm,
     out, branch_out, state_out,
-    wb, wg, wm, normed, gate_act, merged, mix, residual, mall,
+    wb, wg, wm, normed, gate_act, merged, mix, residual, message, mall,
     eg, eu, ed, xall, sbuf, rbuf, obuf, cbuf, pbuf, fbuf, total,
     load_sem, ms, mr, zs, zr, ds_, dr, os_, orr, ps, pr,
 ):
@@ -76,6 +76,13 @@
             device_id_type=pl.DeviceIdType.MESH,
         )
 
+    spots = lax.broadcasted_iota(jnp.int32, (rows, message.shape[1]), 1)
+    wide = jnp.full((rows, message.shape[1]), -1.0, jnp.float32)
+    for k in range(top):
+        wide = jnp.where(spots == k, routes[:, k : k + 1].astype(jnp.float32), wide)
+        wide = jnp.where(spots == top + k, affinity[:, k : k + 1], wide)
+    message[...] = jnp.full(message.shape, -1.0, jnp.float32)
+    message[:, :rows] = jnp.transpose(wide)[: message.shape[0]]
     pl.semaphore_wait(barrier, n - 1)
 
     @pl.loop(1, n)
@@ -104,7 +111,7 @@
 
     for t in range(channels // tile):
         cols = pl.ds(t * tile, tile)
-        conv = pre[:, cols] + branch_out[:, cols].astype(jnp.float32) * tap[:, cols]
+        conv = pre[:, cols] + branch_out[:, cols].astype(jnp.float32) * taps[taps.shape[0] - 1 :, cols]
         conv16 = conv.astype(jnp.bfloat16)
         rate = jax.nn.sigmoid(
             jnp.dot(conv16, spread(rate_b, t), preferred_element_type=jnp.float32)
@@ -112,7 +119,7 @@
         inflow = jax.nn.sigmoid(
             jnp.dot(conv16, spread(input_b, t), preferred_element_type=jnp.float32)
         )
-        log_decay = rate * slope[:, cols]
+        log_decay = rate * (-gate_scale * jax.nn.softplus(-decay_p[:, cols]))
         decay = jnp.exp(log_decay)
         rest = -jnp.tanh(log_decay) * (decay * decay + 1.0)
         state = decay * recur[:, cols] + jnp.sqrt(rest) * (inflow * conv)
@@ -157,13 +164,43 @@
     def seqs(k):
         return pl.ds(pl.multiple_of(k * rows, rows), rows)
 
-    def token_copy(c, d, landing):
-        other, device = along(d)
-        spot = other if landing else plane
+    def token_hop(c, origin, up):
         return rcopy(
-            xall.at[c, seqs(plane)], xall.at[c, seqs(spot)], zs.at[c, other],
-            zr.at[c, spot], device,
-        )
+            xall.at[c, seqs(origin)], xall.at[c, seqs(origin)],
+            zs.at[c, origin + (planes if up else 0)], zr.at[c, origin],
+            lax.rem(me + (group if up else n - group), n),
+        )
+
+    def each_hop(c, step):
+        for up in (True, False):
+            open_end = plane + 1 < planes if up else plane > 0
+            for h in range(planes):
+                origin = plane - h if up else plane + h
+                held = origin >= 0 if up else origin < planes
+
+                @pl.when(open_end & held)
+                def _():
+                    step(token_hop(c, origin, up))
+
+    def own_hops(c):
+        for up in (True, False):
+
+            @pl.when(plane + 1 < planes if up else plane > 0)
+            def _():
+                token_hop(c, plane, up).start()
+
+    def pass_on(c):
+        for h in range(1, planes):
+            for up in (True, False):
+                origin = plane - h if up else plane + h
+
+                @pl.when(origin >= 0 if up else origin < planes)
+                def _():
+                    token_hop(c, origin, up).wait_recv()
+
+                    @pl.when(plane + 1 < planes if up else plane > 0)
+                    def _():
+                        token_hop(c, origin, up).start()
 
     def slab_copy(c, d, landing, src, dst, send, recv):
         other, device = beside(d)
@@ -183,9 +220,9 @@
 
     far = list(range(1, planes))
     near = list(range(1, group))
-    for c in range(parts):
-        for d in far:
-            token_copy(c, d, False).start()
+    ahead = 2
+    for c in range(min(ahead, parts)):
+        own_hops(c)
 
     @pl.loop(1, n)
     def _(d):
@@ -252,8 +289,9 @@
             sums[k] = piece if sums[k] is None else sums[k] + piece
 
     for c in range(parts):
-        for d in far:
-            token_copy(c, d, True).wait_recv()
+        pass_on(c)
+        if c + ahead < parts:
+            own_hops(c + ahead)
         sbuf[c] = jnp.dot(pick, xall[c], preferred_element_type=jnp.float32).astype(jnp.bfloat16)
         for d in near:
             slab_copy(c, d, False, sbuf, rbuf, ds_, dr).start()
@@ -305,8 +343,8 @@
         message_copy(d, False).wait_send()
 
     for c in range(parts):
+        each_hop(c, lambda hop: hop.wait_send())
         for d in far:
-            token_copy(c, d, False).wait_send()
             back_copy(c, d, False).wait_send()
         for d in near:
             slab_copy(c, d, False, sbuf, rbuf, ds_, dr).wait_send()
@@ -338,14 +376,9 @@
     slab = -(-planes * capacity // 16) * 16
     slots, lots, part = group * slab, planes * rows, width // chunks
 
-    message = jnp.concatenate([routes.T.astype(f32), affinity.T], axis=0)
-    message = jnp.pad(
-        message, ((0, -2 * top % 8), (0, -rows % 128)), constant_values=-1.0
-    )
-
     row = lambda v: v.reshape(1, -1)
     pre = jnp.sum(conv_state.astype(f32) * conv_taps[None, :-1], axis=1)
-    slope = row(-gate_scale * jax.nn.softplus(-decay_param))
+    letter = (-(-2 * top // 8) * 8, -(-rows // 128) * 128)
     block = rate_blocks.shape[1]
     dma = lambda *count: pltpu.SemaphoreType.DMA(count)
     layer_out, branch, state_next = pl.pallas_call(
@@ -355,7 +388,7 @@
             jax.ShapeDtypeStruct((rows, channels), bf16),
             jax.ShapeDtypeStruct((rows, channels), f32),
         ),
-        in_specs=vmem(12) + anywhere(6),
+        in_specs=vmem(13) + anywhere(6),
         out_specs=tuple(vmem(3)),
         scratch_shapes=[
             pltpu.VMEM((width, channels), bf16),
@@ -366,7 +399,8 @@
             pltpu.VMEM((rows, channels), bf16),
             pltpu.VMEM((rows, width), f32),
             pltpu.VMEM((rows, width), f32),
-            pltpu.VMEM((message.shape[0], n * message.shape[1]), f32),
+            pltpu.VMEM(letter, f32),
+            pltpu.VMEM((letter[0], n * letter[1]), f32),
             pltpu.VMEM((width, hidden), bf16),
             pltpu.VMEM((width, hidden), bf16),
             pltpu.VMEM((hidden, width), bf16),
@@ -379,16 +413,16 @@
             pltpu.VMEM((chunks, lots, part), bf16),
             pltpu.VMEM((chunks, rows, part), f32),
             dma(6), dma(n), dma(n),
-            dma(chunks, planes), dma(chunks, planes), dma(chunks, group), dma(chunks, group),
+            dma(chunks, 2 * planes), dma(chunks, planes), dma(chunks, group), dma(chunks, group),
             dma(chunks, group), dma(chunks, group), dma(chunks, planes), dma(chunks, planes),
         ],
         compiler_params=pltpu.CompilerParams(
             collective_id=0, has_side_effects=True, vmem_limit_bytes=60 << 20
         ),
     )(
-        tokens, pre, conv_taps[-1:], recur_state, rate_blocks.reshape(channels, block),
-        input_blocks.reshape(channels, block), slope, row(gain_pre), row(gain_post),
-        row(gain_ffn), row(gain_out), message,
+        tokens, pre, conv_taps, recur_state, rate_blocks.reshape(channels, block),
+        input_blocks.reshape(channels, block), row(decay_param), row(gain_pre), row(gain_post),
+        row(gain_ffn), row(gain_out), routes, affinity,
         w_branch, w_gate, w_mix, w_expert_gate, w_expert_up, w_expert_down,
     )
     conv_next = jnp.concatenate([conv_state[:, 1:], branch[:, None, :]], axis=1)

time: 90.4 us -> 87.7 us (0.970)
  other arithmetic: 6.75 us -> 3.49 us
  local copies, waits for them, and re-layouts: 4.66 us -> 6.11 us
    unnamed x2 -> x4, local copies, waits for them, and re-layouts: 3.34 us -> 6.1 us
    slice x1 -> x0, local copies, waits for them, and re-layouts: 1.31 us -> none  [shards(): conv_taps[-1:]]
    mul x1 -> x0, other arithmetic: 1.3 us -> none  [shards(): slope = row(-gate_scale * jax.nn.softplus(-decay_param))]
    concatenate x1 -> x0, other arithmetic: 1.28 us -> none  [shards(): message = jnp.concatenate([routes.T.astype(f32), affinity.T], axis=0)]
where the time goes in v3:
time: 87.7 us; the launch traced here: 87.4 us
  Pallas kernels  77.1 us (88%)
  local copies, waits for them, and re-layouts  6.11 us (7%)
  other arithmetic  3.49 us (4%)
    pallas_call x1, Pallas kernels, shards(): pl.pallas_call(functools.partial(layer_kernel, n, capacity, limit, top),...  77.1 us
    unnamed x4, local copies, waits for them, and re-layouts  6.1 us
    reduce_sum x1, other arithmetic, shards(): pre = jnp.sum(conv_state.astype(f32) * conv_taps[None, :-1], axis=1)  1.8 us

profile of v3, /device:TPU:0, one launch (start us, length us, event | category | flops | bytes accessed | tf_op | source)
XLA Modules:
  0.0 87.4 jit_solution(4617836840365076555)
XLA Ops:
  0.6 1.4 %copy.22.routes = s32[64,2]{1,0:T(8,128)} copy(s32[64,2]{0,1:T(2,128)} %param.33) | data formatting | bytes 1024 | tf_op args[14]
  2.0 1.4 %copy.23.affinity = f32[64,2]{1,0:T(8,128)} copy(f32[64,2]{0,1:T(2,128)} %param.34) | data formatting | bytes 1024 | tf_op args[15]
  3.4 1.8 %multiply_reduce_fusion.pre = f32[64,1024]{1,0:T(8,128)} fusion(bf16[64,3,1024]{2,0,1:T(8,128)(2,1)} %param.20, f32[3,1024]{1,0:T(4,128)} %bitcast.12), kind=kLoop, calls=%fused_computation | loop fusion | flops 524288 | bytes 667648 | tf_op jit(solution)/shard_map/reduce_sum | solution.py:380
  5.2 0.0 slice-start
  5.2 77.1 %shard_map.202 = (bf16[64,2048]{1,0:T(8,128)(2,1)}, bf16[64,1024]{1,0:T(8,128)(2,1)}, f32[64,1024]{1,0:T(8,128)}) custom-call(bf16[64,2048]{1,0:T(8,128)(2,1)} %tokens.1, f32[64,1024]{1,0:T(8,128)} %multiply_reduce_fusion.pre, f32[4,1024]{1,0:T(4,128)} %taps.1, f32[64,1024]{1,0:T(8,128)} %recur.1, bf16[1024,64]{1,0:T(8,128)(2,1)} %bitcast.9, ...), custom_call_target="tpu_custom_call" | custom-call | tf_op jit(solution)/shard_map/pallas_call | solution.py:384
  82.3 0.0 slice-done
  82.4 1.7 %pad_maximum_fusion = bf16[64,3,1024]{2,0,1:T(8,128)(2,1)} fusion(bf16[64,1,1024]{2,0,1:T(8,128)(2,1)} %bitcast.11, bf16[64,2,1024]{2,0,1:T(8,128)(2,1)S(1)} %slice-done), kind=kLoop, calls=%fused_computation.1 | loop fusion | flops 196608 | bytes 786432 | tf_op jit(solution)/shard_map/concatenate | solution.py:428
  84.0 1.7 %copy.26 = bf16[64,2048]{1,0:T(8,128)(2,1)} copy(bf16[64,2048]{1,0:T(8,128)(2,1)} %get-tuple-element.12) | data formatting | bytes 524288
  85.7 1.7 %copy.27 = f32[64,1024]{1,0:T(8,128)} copy(f32[64,1024]{1,0:T(8,128)} %get-tuple-element.14) | data formatting | bytes 524288
Async XLA Ops:
  5.2 77.1 %slice-start = ((bf16[64,3,1024]{2,0,1:T(8,128)(2,1)}), bf16[64,2,1024]{2,0,1:T(8,128)(2,1)S(1)}, s32[]{:S(2)}) async-start(bf16[64,3,1024]{2,0,1:T(8,128)(2,1)} %param.20), calls=%async_computation | async-start | bytes 524288 | tf_op jit(solution)/shard_map/slice | solution.py:428
